TPU v7x, 32 devices: a whole 2x2x4 slice. The times are simulated.
32 devices in a mesh: fs: 16 (over z, y, x), tp: 2 (over core).
Axes of the slice: x: 2, y: 2, z: 4, core: 2. Of those that a mesh axis runs over, the one named last changes fastest.
Arguments:
- tokens: bfloat16 [4096, 2048], P('fs'), may hold values from -6 to 6
- routes: int32 [4096, 6], P('fs'), may hold values from 0 to 15, all different within a row; in each aligned block of 256 rows (0 to 255, 256 to 511, ...) at most 160 rows name the same one
- route_weights: float32 [4096, 6], P('fs'), may hold values from 0.1 to 1
- norm_gain: float32 [2048], P('fs'), may hold values from 0.1 to 1.9
- expert_gate: float32 [16, 2048, 1024], P(None, 'fs', 'tp'), may hold values from -0.125 to 0.125
- expert_up: float32 [16, 2048, 1024], P(None, 'fs', 'tp'), may hold values from -0.125 to 0.125
- expert_down: float32 [16, 2048, 1024], P(None, 'fs', 'tp'), may hold values from -0.1875 to 0.1875
- shared_gate: float32 [2048, 1024], P('fs', 'tp'), may hold values from -0.125 to 0.125
- shared_up: float32 [2048, 1024], P('fs', 'tp'), may hold values from -0.125 to 0.125
- shared_down: float32 [2048, 1024], P('fs', 'tp'), may hold values from -0.1875 to 0.1875
Outputs:
- layer_output: bfloat16 [4096, 2048], P('fs', 'tp')
- sample_gate: bfloat16 [16, 2048, 1024], P('fs', None, 'tp')
- sample_up: bfloat16 [16, 2048, 1024], P('fs', None, 'tp')
- sample_down: bfloat16 [16, 2048, 1024], P('fs', None, 'tp')
- common_gate: bfloat16 [2048, 1024], P(None, 'tp')
- common_up: bfloat16 [2048, 1024], P(None, 'tp')
- common_down: bfloat16 [2048, 1024], P(None, 'tp')
Inputs may be any that keep to these rules, and one draw needn't show every extreme that they name: `routes`: each row names 6 different experts. In each aligned block of 256 rows (the rows of one index of fs) no expert is named by more than 160 rows, a bound that some expert reaches in some blocks.
All inputs are finite; a program needn't handle non-finite values.
Results may differ from a plain program's by a relative error of at most 0.015.
Values may be sent and summed in bfloat16 or wider, within the bound.
A program may use at most 128 MiB of HBM per device.

v0:
```python
import jax
import jax.numpy as jnp
from jax import lax
from jax.sharding import PartitionSpec as P

EPSILON = 1e-06


def normalize(tokens):
    values = tokens.astype(jnp.float32)
    scale = lax.rsqrt(jnp.mean(values * values, axis=-1, keepdims=True) + EPSILON)
    return (values * scale).astype(jnp.bfloat16)


def body(
    tokens,
    routes,
    route_weights,
    norm_gain,
    expert_gate,
    expert_up,
    expert_down,
    shared_gate,
    shared_up,
    shared_down,
):
    tp_count = lax.axis_size("tp")
    tp_index = lax.axis_index("tp")
    fs_count = lax.axis_size("fs")
    tok_rows, width = tokens.shape
    experts = expert_gate.shape[0]
    share = tok_rows // tp_count
    own_experts = experts // fs_count
    normed = normalize(tokens)
    own_normed = lax.dynamic_slice_in_dim(normed, tp_index * share, share, 0)
    own_routes = lax.dynamic_slice_in_dim(routes, tp_index * share, share, 0)
    own_weights = lax.dynamic_slice_in_dim(route_weights, tp_index * share, share, 0)
    member = own_routes[None, :, :] == jnp.arange(experts, dtype=jnp.int32)[:, None, None]
    dense = jnp.sum(jnp.where(member, own_weights[None, :, :], 0.0), axis=2)
    gathered = lax.all_gather(own_normed, "fs", axis=0, tiled=True)
    dense_all = lax.all_gather(dense, "fs", axis=0, tiled=False)
    gain_rows = norm_gain[None, :, None]
    rounded = (
        (expert_gate * gain_rows).astype(jnp.bfloat16),
        (expert_up * gain_rows).astype(jnp.bfloat16),
        expert_down.astype(jnp.bfloat16),
    )
    sample_gate, sample_up, sample_down = (
        lax.all_to_all(rounded[0], "fs", split_axis=0, concat_axis=1, tiled=True),
        lax.all_to_all(rounded[1], "fs", split_axis=0, concat_axis=1, tiled=True),
        lax.all_to_all(rounded[2], "fs", split_axis=0, concat_axis=1, tiled=True),
    )
    common_gate, common_up, common_down = (
        lax.all_gather(
            (shared_gate * norm_gain[:, None]).astype(jnp.bfloat16), "fs", axis=0, tiled=True
        ),
        lax.all_gather(
            (shared_up * norm_gain[:, None]).astype(jnp.bfloat16), "fs", axis=0, tiled=True
        ),
        lax.all_gather(shared_down.astype(jnp.bfloat16), "fs", axis=0, tiled=True),
    )
    shared_gate_act = jnp.dot(normed, common_gate, preferred_element_type=jnp.float32)
    shared_up_act = jnp.dot(normed, common_up, preferred_element_type=jnp.float32)
    shared_hidden = (jax.nn.silu(shared_gate_act) * shared_up_act).astype(jnp.bfloat16)
    shared_part = jnp.einsum(
        "th,dh->td", shared_hidden, common_down, preferred_element_type=jnp.float32
    ).astype(jnp.bfloat16)
    shared_parts = lax.all_to_all(
        shared_part.reshape(tok_rows, tp_count, width // tp_count).transpose(1, 0, 2),
        "tp",
        split_axis=0,
        concat_axis=0,
        tiled=True,
    )
    shared_sum = jnp.sum(shared_parts.astype(jnp.float32), axis=0)
    scale_all = lax.dynamic_slice_in_dim(
        dense_all, lax.axis_index("fs") * own_experts, own_experts, 1
    )
    total = None
    for expert in range(own_experts):
        scale = scale_all[:, expert, :].reshape(-1)[:, None]
        for shift in range(tp_count):
            gate_w, up_w, down_w = (sample_gate[expert], sample_up[expert], sample_down[expert])
            if shift:
                ring = [(i, (i + shift) % tp_count) for i in range(tp_count)]
                gate_w, up_w, down_w = (
                    lax.ppermute(gate_w, "tp", ring),
                    lax.ppermute(up_w, "tp", ring),
                    lax.ppermute(down_w, "tp", ring),
                )
            gate = jnp.dot(gathered, gate_w, preferred_element_type=jnp.float32)
            upward = jnp.dot(gathered, up_w, preferred_element_type=jnp.float32)
            hidden = (jax.nn.silu(gate) * upward * scale).astype(jnp.bfloat16)
            part = jnp.einsum("rf,df->rd", hidden, down_w, preferred_element_type=jnp.float32)
            total = part if total is None else total + part
    routed = lax.psum_scatter(total.astype(jnp.bfloat16), "fs", scatter_dimension=0, tiled=True)
    routed = lax.all_to_all(routed, "tp", split_axis=1, concat_axis=0, tiled=True)
    layer_output = (routed.astype(jnp.float32) + shared_sum).astype(jnp.bfloat16)
    return (layer_output, sample_gate, sample_up, sample_down, common_gate, common_up, common_down)


def solution(mesh):
    return jax.shard_map(
        body,
        mesh=mesh,
        in_specs=(
            P("fs", None),
            P("fs", None),
            P("fs", None),
            P("fs"),
            P(None, "fs", "tp"),
            P(None, "fs", "tp"),
            P(None, "fs", "tp"),
            P("fs", "tp"),
            P("fs", "tp"),
            P("fs", "tp"),
        ),
        out_specs=(
            P("fs", "tp"),
            P("fs", None, "tp"),
            P("fs", None, "tp"),
            P("fs", None, "tp"),
            P(None, "tp"),
            P(None, "tp"),
            P(None, "tp"),
        ),
        check_vma=False,
    )
```

profile of v0, /device:TPU:11, one launch (start us, length us, event | category | flops | bytes accessed | tf_op | source)
XLA Modules:
  0.0 607.8 jit_solution(15371878558450184911)
XLA Ops:
  7.2 0.0 all-gather.6.cloned.1.call-start
  7.2 1.5 fusion
  8.8 1.5 fusion.1
  10.2 0.8 constant_dynamic-slice_fusion.3
  11.1 0.0 all-gather.6.cloned.1.call-update
  11.1 6.8 %multiply_convert_fusion.2 = (bf16[16,128,512]{2,1,0:T(8,128)(2,1)}, bf16[16,128,512]{2,1,0:T(8,128)(2,1)}) fusion(f32[16,128,512]{2,1,0:T(8,128)} %param.15, f32[128]{0:T(128)S(1)} %copy-done.8, f32[16,128,512]{2,1,0:T(8,128)} %param.14), kind=kLoop, calls=%fused_computation.3 | loop fusion | flops 4194304 | bytes 12583424 | tf_op jit(solution)/shard_map/convert_element_type | solution.py:45
  17.9 6.8 %all-to-all-start = ((bf16[16,128,512]{2,1,0:T(8,128)(2,1)}), bf16[16,128,512]{2,1,0:T(8,128)(2,1)S(1)}, u32[]{:S(2)}, u32[]{:S(2)}) async-start(bf16[16,128,512]{2,1,0:T(8,128)(2,1)} %get-tuple-element.8), calls=%async_computation | async-start | bytes 4194304 | tf_op jit(solution)/shard_map/all_to_all | solution.py:49
  24.7 0.0 all-gather.8.cloned.1.call-start
  24.7 1.8 multiply_convert_fusion.6
  26.5 74.4 %all-to-all-done = bf16[16,128,512]{2,1,0:T(8,128)(2,1)S(1)} async-done(((bf16[16,128,512]{2,1,0:T(8,128)(2,1)}), bf16[16,128,512]{2,1,0:T(8,128)(2,1)S(1)}, u32[]{:S(2)}, u32[]{:S(2)}) %all-to-all-start) | async-done | bytes 2097184 | tf_op jit(solution)/shard_map/all_to_all | solution.py:49
  101.0 6.9 %all-to-all-start.1 = ((bf16[16,128,512]{2,1,0:T(8,128)(2,1)}), bf16[16,128,512]{2,1,0:T(8,128)(2,1)}, u32[]{:S(2)}, u32[]{:S(2)}) async-start(bf16[16,128,512]{2,1,0:T(8,128)(2,1)} %get-tuple-element.7), calls=%async_computation.1 | async-start | bytes 4194304 | tf_op jit(solution)/shard_map/all_to_all | solution.py:50
  107.8 0.0 all-gather.10.cloned.1.call-start
  107.9 0.7 all-gather.10.cloned.1.call-update
  108.6 3.9 convert_element_type.59
  112.5 81.0 %all-to-all-done.1 = bf16[16,128,512]{2,1,0:T(8,128)(2,1)} async-done(((bf16[16,128,512]{2,1,0:T(8,128)(2,1)}), bf16[16,128,512]{2,1,0:T(8,128)(2,1)}, u32[]{:S(2)}, u32[]{:S(2)}) %all-to-all-start.1) | async-done | bytes 2097184 | tf_op jit(solution)/shard_map/all_to_all | solution.py:50
  193.5 9.3 %all-to-all-start.2 = ((bf16[16,128,512]{2,1,0:T(8,128)(2,1)}), bf16[16,128,512]{2,1,0:T(8,128)(2,1)}, u32[]{:S(2)}, u32[]{:S(2)}) async-start(bf16[16,128,512]{2,1,0:T(8,128)(2,1)} %convert_element_type.59), calls=%async_computation.2 | async-start | bytes 4194304 | tf_op jit(solution)/shard_map/all_to_all | solution.py:51
  202.8 0.0 all-gather.12.cloned.1.call-start
  202.8 4.0 collective-permute-start
  206.9 0.7 convert_element_type.68
  207.5 0.0 all-gather.12.cloned.1.call-update
  207.5 0.0 reduce-scatter.2.cloned.1.call-start
  207.7 68.8 %all-gather = f32[256,128]{1,0:T(8,128)S(1)} all-gather(f32[16,128]{1,0:T(8,128)S(1)} %select_reduce_fusion), channel_id=2, replica_groups=mesh['fs'=16,'tp'=2] {'fs'}, dimensions={0}, use_global_device_ids=true | all-gather | bytes 139264 | tf_op jit(solution)/shard_map/all_gather | solution.py:41
  276.5 8.9 %collective-permute-start.1 = (bf16[2048,512]{1,0:T(8,128)(2,1)}, bf16[2048,512]{1,0:T(8,128)(2,1)}, u32[]{:S(2)}, u32[]{:S(2)}) collective-permute-start(bf16[2048,512]{1,0:T(8,128)(2,1)} %bitcast.1), channel_id=1, source_target_pairs={{0,1},{1,0},{2,3},{3,2},{4,5},{5,4},{6,7},{7,6},{8,9},{9,8},{10,11... | collective-permute-start | bytes 6291464 | tf_op jit(solution)/shard_map/ppermute | solution.py:88
  285.4 0.1 collective-permute-start.2
  285.5 9.8 %fusion.16 = f32[2048,512]{1,0:T(8,128)} fusion(bf16[2048,2048]{1,0:T(8,128)(2,1)} %all-gather.6.cloned.1.call-done, bf16[2048,512]{1,0:T(8,128)(2,1)S(1)} %bitcast.41), kind=kOutput, calls=%fused_computation.38 | convolution fusion | flops 4294967296 | bytes 14680064 | tf_op jit(solution)/shard_map/dot_general | solution.py:91
  295.3 7.6 %fusion.17 = f32[2048,512]{1,0:T(8,128)} fusion(bf16[2048,2048]{1,0:T(8,128)(2,1)S(1)} %copy-done.9, bf16[2048,512]{1,0:T(8,128)(2,1)} %collective-permute-done), kind=kOutput, calls=%fused_computation.39 | convolution fusion | flops 4294967296 | bytes 14680064 | tf_op jit(solution)/shard_map/dot_general | solution.py:91
  302.9 7.6 %fusion.18 = f32[2048,512]{1,0:T(8,128)} fusion(bf16[2048,2048]{1,0:T(8,128)(2,1)S(1)} %copy-done.9, bf16[2048,512]{1,0:T(8,128)(2,1)} %collective-permute-done.1), kind=kOutput, calls=%fused_computation.40 | convolution fusion | flops 4294967296 | bytes 14680064 | tf_op jit(solution)/shard_map/dot_general | solution.py:92
  310.5 16.6 %fusion.6 = f32[2048,2048]{1,0:T(8,128)} fusion(bf16[2048,512]{1,0:T(8,128)(2,1)} %bitcast.4, f32[2048,512]{1,0:T(8,128)} %fusion.16, bf16[2048,2048]{1,0:T(8,128)(2,1)} %all-gather.6.cloned.1.call-done, bf16[2048,512]{1,0:T(8,128)(2,1)} %bitcast.1, f32[2048]{0:T(1024)S(1)} %bitcast.48), kind=kOutput, calls=%fused_computation.18 | convolution fusion | flops 8597274624 | bytes 33562624 | tf_op jit(solution)/shard_map/rf,df->rd/dot_general | solution.py:94
  327.0 13.6 %add_convert_fusion = bf16[2048,2048]{1,0:T(8,128)(2,1)} fusion(f32[2048,2048]{1,0:T(8,128)} %fusion.6, bf16[2048,512]{1,0:T(8,128)(2,1)} %collective-permute-done.2, f32[2048,512]{1,0:T(8,128)} %fusion.18, f32[2048,512]{1,0:T(8,128)} %fusion.17, f32[2048]{0:T(1024)S(1)} %bitcast.49), kind=kOutput, calls=%fused_computation | convolution fusion | flops 4310695936 | bytes 35659776 | tf_op jit(solution)/shard_map/rf,df->rd/dot_general | solution.py:94
  340.6 0.0 reduce-scatter.2.cloned.1.call-update
  340.6 0.0 all-gather.8.cloned.1.call-done
  340.7 3.1 fusion.19
  343.8 55.0 %all-gather.12.cloned.1.call-done = bf16[2048,512]{1,0:T(8,128)(2,1)} async-done(((bf16[128,512]{1,0:T(8,128)(2,1)}), bf16[2048,512]{1,0:T(8,128)(2,1)}) %all-gather.12.cloned.1.call-update) | async-done | bytes 2097168 | tf_op jit(solution)/shard_map/all_gather | solution.py:60
  398.8 4.7 convolution_convert_fusion
  403.5 2.3 copy.30
  405.7 5.2 all-to-all-start.4
  410.9 1.7 all-to-all-done.4
  412.7 1.2 convert_reduce_fusion
  413.9 167.8 %reduce-scatter.2.cloned.1.call-done = bf16[128,2048]{1,0:T(8,128)(2,1)} async-done(((bf16[2048,2048]{1,0:T(8,128)(2,1)}), bf16[128,2048]{1,0:T(8,128)(2,1)}) %reduce-scatter.2.cloned.1.call-update) | async-done | bytes 524304 | tf_op jit(solution)/shard_map/reduce_scatter | solution.py:96
  581.7 1.1 copy.31
  582.8 4.7 all_to_all.54
  587.4 2.2 fusion.5
  589.6 1.3 copy.38
  590.9 3.2 copy.39
  594.1 3.2 copy.40
  597.3 1.3 copy.41
  598.7 1.3 copy.42
  600.0 1.3 copy.43
  (32 shorter events, 0.1 us)
Async XLA Ops:
  7.2 200.4 %copy-start = (f32[256,6]{0,1:T(8,128)S(1)}, f32[256,6]{0,1:T(8,128)}, u32[]{:S(2)}) copy-start(f32[256,6]{0,1:T(8,128)} %param.12) | copy-start | bytes 18436
  7.2 3.9 copy-start.8
  7.2 278.3 %all-gather.6.cloned.1.call-start = ((), (), s32[]{:S(2)}) async-start(), calls=%async_computation.6 | async-start | bytes 8912896 | tf_op jit(solution)/shard_map/all_gather | solution.py:40
  17.9 6.8 %copy-start.6 = (f32[128,512]{1,0:T(8,128)S(1)}, f32[128,512]{1,0:T(8,128)}, u32[]{:S(2)}) copy-start(f32[128,512]{1,0:T(8,128)} %param.17) | copy-start | bytes 786436
  17.9 83.0 %all-to-all-start = ((bf16[16,128,512]{2,1,0:T(8,128)(2,1)}), bf16[16,128,512]{2,1,0:T(8,128)(2,1)S(1)}, u32[]{:S(2)}, u32[]{:S(2)}) async-start(bf16[16,128,512]{2,1,0:T(8,128)(2,1)} %get-tuple-element.8), calls=%async_computation | async-start | bytes 4194304 | tf_op jit(solution)/shard_map/all_to_all | solution.py:49
  24.7 316.0 %all-gather.8.cloned.1.call-start = ((), (), s32[]{:S(2)}) async-start(), calls=%async_computation.8 | async-start | bytes 2228224 | tf_op jit(solution)/shard_map/all_gather | solution.py:54
  101.0 92.5 %all-to-all-start.1 = ((bf16[16,128,512]{2,1,0:T(8,128)(2,1)}), bf16[16,128,512]{2,1,0:T(8,128)(2,1)}, u32[]{:S(2)}, u32[]{:S(2)}) async-start(bf16[16,128,512]{2,1,0:T(8,128)(2,1)} %get-tuple-element.7), calls=%async_computation.1 | async-start | bytes 4194304 | tf_op jit(solution)/shard_map/all_to_all | solution.py:50
  107.8 235.9 %all-gather.10.cloned.1.call-start = ((), (), s32[]{:S(2)}) async-start(), calls=%async_computation.9 | async-start | bytes 2228224 | tf_op jit(solution)/shard_map/all_gather | solution.py:57
  108.6 98.3 %copy-start.5 = (f32[128,512]{1,0:T(8,128)S(1)}, f32[128,512]{1,0:T(8,128)}, u32[]{:S(2)}) copy-start(f32[128,512]{1,0:T(8,128)} %param.19) | copy-start | bytes 786436
  108.6 99.1 %copy-start.7 = (s32[256,6]{0,1:T(8,128)S(1)}, s32[256,6]{0,1:T(8,128)}, u32[]{:S(2)}) copy-start(s32[256,6]{0,1:T(8,128)} %param.11) | copy-start | bytes 18436
  193.5 91.9 %all-to-all-start.2 = ((bf16[16,128,512]{2,1,0:T(8,128)(2,1)}), bf16[16,128,512]{2,1,0:T(8,128)(2,1)}, u32[]{:S(2)}, u32[]{:S(2)}) async-start(bf16[16,128,512]{2,1,0:T(8,128)(2,1)} %convert_element_type.59), calls=%async_computation.2 | async-start | bytes 4194304 | tf_op jit(solution)/shard_map/all_to_all | solution.py:51
  202.8 196.0 %all-gather.12.cloned.1.call-start = ((), (), s32[]{:S(2)}) async-start(), calls=%async_computation.10 | async-start | bytes 2228224 | tf_op jit(solution)/shard_map/all_gather | solution.py:60
  202.8 92.5 %collective-permute-start = (bf16[2048,512]{1,0:T(8,128)(2,1)S(1)}, bf16[2048,512]{1,0:T(8,128)(2,1)}, u32[]{:S(2)}, u32[]{:S(2)}) collective-permute-start(bf16[2048,512]{1,0:T(8,128)(2,1)S(1)} %bitcast.40), channel_id=1, source_target_pairs={{0,1},{1,0},{2,3},{3,2},{4,5},{5,4},{6,7},{7,6},{8,9},{9,8},{10,11... | collective-permute-start | bytes 6291464 | tf_op jit(solution)/shard_map/ppermute | solution.py:87
  207.5 374.1 %reduce-scatter.2.cloned.1.call-start = ((), (), s32[]{:S(2)}) async-start(), calls=%async_computation.7 | async-start | bytes 8912896 | tf_op jit(solution)/shard_map/reduce_scatter | solution.py:96
  276.5 26.4 %collective-permute-start.1 = (bf16[2048,512]{1,0:T(8,128)(2,1)}, bf16[2048,512]{1,0:T(8,128)(2,1)}, u32[]{:S(2)}, u32[]{:S(2)}) collective-permute-start(bf16[2048,512]{1,0:T(8,128)(2,1)} %bitcast.1), channel_id=1, source_target_pairs={{0,1},{1,0},{2,3},{3,2},{4,5},{5,4},{6,7},{7,6},{8,9},{9,8},{10,11... | collective-permute-start | bytes 6291464 | tf_op jit(solution)/shard_map/ppermute | solution.py:88
  285.4 41.6 %collective-permute-start.2 = (bf16[2048,512]{1,0:T(8,128)(2,1)}, bf16[2048,512]{1,0:T(8,128)(2,1)}, u32[]{:S(2)}, u32[]{:S(2)}) collective-permute-start(bf16[2048,512]{1,0:T(8,128)(2,1)} %bitcast.4), channel_id=1, source_target_pairs={{0,1},{1,0},{2,3},{3,2},{4,5},{5,4},{6,7},{7,6},{8,9},{9,8},{10,11... | collective-permute-start | bytes 6291464 | tf_op jit(solution)/shard_map/ppermute | solution.py:89
  285.5 9.8 %copy-start.9 = (bf16[2048,2048]{1,0:T(8,128)(2,1)S(1)}, bf16[2048,2048]{1,0:T(8,128)(2,1)}, u32[]{:S(2)}) copy-start(bf16[2048,2048]{1,0:T(8,128)(2,1)} %all-gather.6.cloned.1.call-done) | copy-start | bytes 25165828
  405.7 6.9 %all-to-all-start.4 = ((bf16[2,256,1024]{2,1,0:T(8,128)(2,1)}), bf16[2,256,1024]{2,1,0:T(8,128)(2,1)S(1)}, u32[]{:S(2)}, u32[]{:S(2)}) async-start(bf16[2,256,1024]{2,1,0:T(8,128)(2,1)} %bitcast.43), calls=%async_computation.5 | async-start | bytes 2097152 | tf_op jit(solution)/shard_map/all_to_all | solution.py:68
  590.9 6.4 %copy-start.2 = (bf16[2048,512]{1,0:T(8,128)(2,1)S(1)}, bf16[2048,512]{1,0:T(8,128)(2,1)}, u32[]{:S(2)}) copy-start(bf16[2048,512]{1,0:T(8,128)(2,1)} %all-gather.8.cloned.1.call-done) | copy-start | bytes 6291460
  594.1 4.5 copy-start.3
  597.3 2.6 copy-start.4
  597.3 4.0 copy-start.1
Sparse Core Ops, SparseCore 0:
  11.3 187.2 all-gather.5
  202.0 71.4 all-gather.7
  276.8 59.5 all-gather.9
  339.6 59.1 all-gather.11
  400.9 180.7 reduce-scatter.1
where the time goes:
time: 609 us; the launch traced here: 608 us
  waiting for transfers between devices  381 us (63%)
  blocking collectives  73.5 us (12%)
  matrix products  62.9 us (10%)
  starting transfers between devices  41.3 us (7%)
  other arithmetic  19.5 us (3%)
  local copies, waits for them, and re-layouts  15.9 us (3%)
  between operations  13.9 us (2%)
    reduce_scatter x1, waiting for transfers between devices, body(): lax.psum_scatter(total.astype(jnp.bfloat16), 'fs', scatter_dimension=0, t...  168 us
    all_to_all x1, waiting for transfers between devices, body(): lax.all_to_all(rounded[1], 'fs', split_axis=0, concat_axis=1, tiled=True)  81 us
    all_to_all x1, waiting for transfers between devices, body(): lax.all_to_all(rounded[0], 'fs', split_axis=0, concat_axis=1, tiled=True)  74.4 us
    all_gather x1, blocking collectives, body(): dense_all = lax.all_gather(dense, 'fs', axis=0, tiled=False)  68.8 us
    all_gather x1, waiting for transfers between devices, body(): lax.all_gather(shared_down.astype(jnp.bfloat16), 'fs', axis=0, tiled=True)  55 us
    dot_general x2, matrix products, body(): jnp.einsum('rf,df->rd', hidden, down_w, preferred_element_type=jnp.float32)  30.1 us
    dot_general x2, matrix products, body(): gate = jnp.dot(gathered, gate_w, preferred_element_type=jnp.float32)  17.4 us
  transfers between devices with their start and end apart: 12, of which 5 were waited for; matrix products, arithmetic and copies ran while one was open for 13% of the time, Pallas kernels for 0%

commit v1 on v0

--- a/solution.py
+++ b/solution.py
@@ -4,6 +4,28 @@
 from jax.sharding import PartitionSpec as P
 
 EPSILON = 1e-06
+
+
+def joined_along(blocks, dim):
+    blocks = jnp.moveaxis(blocks, 0, dim)
+    shape = blocks.shape
+    return blocks.reshape(*shape[:dim], shape[dim] * shape[dim + 1], *shape[dim + 2 :])
+
+
+def collect(value, axis, dim):
+    length = lax.axis_size(axis)
+    pairs = [(i, (i + 1) % length) for i in range(length)]
+    back = [(b, a) for a, b in pairs]
+    lower, upper = ([], [])
+    for lap in range(length - 1):
+        if lap % 2 == 0:
+            lower.append(lax.ppermute(lower[-1] if lower else value, axis, pairs))
+        else:
+            upper.append(lax.ppermute(upper[-1] if upper else value, axis, back))
+    blocks = jnp.stack([*lower[::-1], value, *upper])
+    shift = lax.axis_index(axis) - len(lower)
+    blocks = blocks[(jnp.arange(length) - shift) % length]
+    return joined_along(blocks, dim)
 
 
 def normalize(tokens):
@@ -57,7 +79,7 @@
         lax.all_gather(
             (shared_up * norm_gain[:, None]).astype(jnp.bfloat16), "fs", axis=0, tiled=True
         ),
-        lax.all_gather(shared_down.astype(jnp.bfloat16), "fs", axis=0, tiled=True),
+        collect(shared_down.astype(jnp.bfloat16), "fs", 0),
     )
     shared_gate_act = jnp.dot(normed, common_gate, preferred_element_type=jnp.float32)
     shared_up_act = jnp.dot(normed, common_up, preferred_element_type=jnp.float32)

time: 609 us -> 586 us (0.962)
  waiting for transfers between devices: 381 us -> 249 us
  blocking collectives: 73.5 us -> 163 us
  local copies, waits for them, and re-layouts: 15.9 us -> 39.2 us
    reduce_scatter x1, waiting for transfers between devices: 168 us -> 77.6 us  [body(): lax.psum_scatter(total.astype(jnp.bfloat16), 'fs', scatter_dimension=0, t...]
    ppermute x0 -> x15, waiting for transfers between devices: none -> 88.3 us  [the longest x8 56.5 us: collect(): lower.append(lax.ppermute(lower[-1] if lower else value, axis, pairs))]
    all_to_all x0 -> x1, blocking collectives: none -> 85.9 us  [body(): lax.all_to_all(rounded[0], 'fs', split_axis=0, concat_axis=1, tiled=True)]
    all_to_all x1 -> x0, waiting for transfers between devices: 74.4 us -> none  [body(): lax.all_to_all(rounded[0], 'fs', split_axis=0, concat_axis=1, tiled=True)]
    all_gather x1 -> x0, waiting for transfers between devices: 55 us -> none  [body(): lax.all_gather(shared_down.astype(jnp.bfloat16), 'fs', axis=0, tiled=True)]
    unnamed x26 -> x59, local copies, waits for them, and re-layouts: 11.7 us -> 30.7 us
    ppermute x0 -> x15, starting transfers between devices: none -> 14.3 us  [the longest x8 12.3 us: collect(): lower.append(lax.ppermute(lower[-1] if lower else value, axis, pairs))]
    all_to_all x1 -> x0, starting transfers between devices: 6.77 us -> none  [body(): lax.all_to_all(rounded[0], 'fs', split_axis=0, concat_axis=1, tiled=True)]
  transfers between devices with their start and end apart: 12 -> 25, of which waited for: 5 -> 16; matrix products, arithmetic and copies ran while one was open for 13% -> 17% of each run, Pallas kernels for 0% -> 0%
where the time goes in v1:
time: 586 us; the launch traced here: 585 us
  waiting for transfers between devices  249 us (42%)
  blocking collectives  163 us (28%)
  matrix products  63 us (11%)
  starting transfers between devices  39.6 us (7%)
  local copies, waits for them, and re-layouts  39.2 us (7%)
  other arithmetic  17.6 us (3%)
  between operations  14 us (2%)
    all_to_all x1, blocking collectives, body(): lax.all_to_all(rounded[0], 'fs', split_axis=0, concat_axis=1, tiled=True)  85.9 us
    all_to_all x1, waiting for transfers between devices, body(): lax.all_to_all(rounded[1], 'fs', split_axis=0, concat_axis=1, tiled=True)  80.8 us
    reduce_scatter x1, waiting for transfers between devices, body(): lax.psum_scatter(total.astype(jnp.bfloat16), 'fs', scatter_dimension=0, t...  77.6 us
    all_gather x1, blocking collectives, body(): dense_all = lax.all_gather(dense, 'fs', axis=0, tiled=False)  72.3 us
    ppermute x8, waiting for transfers between devices, collect(): lower.append(lax.ppermute(lower[-1] if lower else value, axis, pairs))  56.5 us
    ppermute x7, waiting for transfers between devices, collect(): upper.append(lax.ppermute(upper[-1] if upper else value, axis, back))  31.8 us
    unnamed x59, local copies, waits for them, and re-layouts  30.7 us
    dot_general x2, matrix products, body(): jnp.einsum('rf,df->rd', hidden, down_w, preferred_element_type=jnp.float32)  30.2 us
  transfers between devices with their start and end apart: 25, of which 16 were waited for; matrix products, arithmetic and copies ran while one was open for 17% of the time, Pallas kernels for 0%

profile of v1, /device:TPU:11, one launch (start us, length us, event | category | flops | bytes accessed | tf_op | source)
XLA Modules:
  0.0 584.9 jit_solution(2468014008433568807)
XLA Ops:
  11.1 6.1 %multiply_convert_fusion.2 = (bf16[16,128,512]{2,1,0:T(8,128)(2,1)}, bf16[16,128,512]{2,1,0:T(8,128)(2,1)S(1)}) fusion(f32[16,128,512]{2,1,0:T(8,128)} %param.15, f32[128]{0:T(128)S(1)} %copy-done.18, f32[16,128,512]{2,1,0:T(8,128)} %param.14), kind=kLoop, calls=%fused_computation.4 | loop fusion | flops 4194304 | bytes 12583424 | tf_op jit(solution)/shard_map/convert_element_type | solution.py:67
  17.2 85.9 %all_to_all.54 = bf16[16,128,512]{2,1,0:T(8,128)(2,1)S(1)} all-to-all(bf16[16,128,512]{2,1,0:T(8,128)(2,1)S(1)} %get-tuple-element.8), channel_id=1, replica_groups=mesh['fs'=16,'tp'=2] {'fs'}, dimensions={0} | all-to-all | bytes 4194304 | tf_op jit(solution)/shard_map/all_to_all | solution.py:71
  103.2 5.2 all-to-all-start.1
  108.4 1.8 multiply_convert_fusion.6
  110.2 3.8 convert_element_type.59
  114.0 80.8 %all-to-all-done.1 = bf16[16,128,512]{2,1,0:T(8,128)(2,1)} async-done(((bf16[16,128,512]{2,1,0:T(8,128)(2,1)}), bf16[16,128,512]{2,1,0:T(8,128)(2,1)}, u32[]{:S(2)}, u32[]{:S(2)}) %all-to-all-start.1) | async-done | bytes 2097184 | tf_op jit(solution)/shard_map/all_to_all | solution.py:72
  194.8 7.4 %all-to-all-start.2 = ((bf16[16,128,512]{2,1,0:T(8,128)(2,1)}), bf16[16,128,512]{2,1,0:T(8,128)(2,1)}, u32[]{:S(2)}, u32[]{:S(2)}) async-start(bf16[16,128,512]{2,1,0:T(8,128)(2,1)} %convert_element_type.59), calls=%async_computation.2 | async-start | bytes 4194304 | tf_op jit(solution)/shard_map/all_to_all | solution.py:73
  203.5 72.3 %all-gather = f32[256,128]{1,0:T(8,128)S(1)} all-gather(f32[16,128]{1,0:T(8,128)S(1)} %select_reduce_fusion), channel_id=2, replica_groups=mesh['fs'=16,'tp'=2] {'fs'}, dimensions={0}, use_global_device_ids=true | all-gather | bytes 139264 | tf_op jit(solution)/shard_map/all_gather | solution.py:63
  275.8 6.8 %collective-permute-start.1 = (bf16[2048,512]{1,0:T(8,128)(2,1)}, bf16[2048,512]{1,0:T(8,128)(2,1)}, u32[]{:S(2)}, u32[]{:S(2)}) collective-permute-start(bf16[2048,512]{1,0:T(8,128)(2,1)} %bitcast.1), channel_id=1, source_target_pairs={{0,1},{1,0},{2,3},{3,2},{4,5},{5,4},{6,7},{7,6},{8,9},{9,8},{10,11... | collective-permute-start | bytes 6291464 | tf_op jit(solution)/shard_map/ppermute | solution.py:110
  282.8 9.7 %fusion.18 = f32[2048,512]{1,0:T(8,128)} fusion(bf16[2048,2048]{1,0:T(8,128)(2,1)} %all-gather.5.cloned.1.call-done, bf16[2048,512]{1,0:T(8,128)(2,1)S(1)} %bitcast.76), kind=kOutput, calls=%fused_computation.62 | convolution fusion | flops 4294967296 | bytes 14680064 | tf_op jit(solution)/shard_map/dot_general | solution.py:113
  292.4 7.7 %fusion.19 = f32[2048,512]{1,0:T(8,128)} fusion(bf16[2048,2048]{1,0:T(8,128)(2,1)S(1)} %copy-done.19, bf16[2048,512]{1,0:T(8,128)(2,1)} %collective-permute-done), kind=kOutput, calls=%fused_computation.63 | convolution fusion | flops 4294967296 | bytes 14680064 | tf_op jit(solution)/shard_map/dot_general | solution.py:113
  300.1 7.6 %fusion.20 = f32[2048,512]{1,0:T(8,128)} fusion(bf16[2048,2048]{1,0:T(8,128)(2,1)S(1)} %copy-done.19, bf16[2048,512]{1,0:T(8,128)(2,1)} %collective-permute-done.1), kind=kOutput, calls=%fused_computation.64 | convolution fusion | flops 4294967296 | bytes 14680064 | tf_op jit(solution)/shard_map/dot_general | solution.py:114
  307.7 16.7 %fusion.6 = f32[2048,2048]{1,0:T(8,128)} fusion(bf16[2048,512]{1,0:T(8,128)(2,1)} %bitcast.4, f32[2048,512]{1,0:T(8,128)} %fusion.18, bf16[2048,2048]{1,0:T(8,128)(2,1)} %all-gather.5.cloned.1.call-done, bf16[2048,512]{1,0:T(8,128)(2,1)} %bitcast.1, f32[2048]{0:T(1024)S(1)} %bitcast.85), kind=kOutput, calls=%fused_computation.19 | convolution fusion | flops 8597274624 | bytes 33562624 | tf_op jit(solution)/shard_map/rf,df->rd/dot_general | solution.py:116
  324.4 13.5 %add_convert_fusion = bf16[2048,2048]{1,0:T(8,128)(2,1)} fusion(f32[2048,2048]{1,0:T(8,128)} %fusion.6, bf16[2048,512]{1,0:T(8,128)(2,1)} %collective-permute-done.2, f32[2048,512]{1,0:T(8,128)} %fusion.20, f32[2048,512]{1,0:T(8,128)} %fusion.19, f32[2048]{0:T(1024)S(1)} %bitcast.86), kind=kOutput, calls=%fused_computation.1 | convolution fusion | flops 4310695936 | bytes 35659776 | tf_op jit(solution)/shard_map/rf,df->rd/dot_general | solution.py:116
  338.9 1.8 collective-permute-start.3
  340.7 2.9 collective-permute-done.3
  343.6 2.6 collective-permute-start.4
  346.8 14.7 %collective-permute-done.4 = bf16[128,512]{1,0:T(8,128)(2,1)S(1)} collective-permute-done((bf16[128,512]{1,0:T(8,128)(2,1)S(1)}, bf16[128,512]{1,0:T(8,128)(2,1)S(1)}, u32[]{:S(2)}, u32[]{:S(2)}) %collective-permute-start.4) | collective-permute-done | bytes 131104 | tf_op jit(solution)/shard_map/ppermute | solution.py:22
  363.6 8.7 %collective-permute-done.5 = bf16[128,512]{1,0:T(8,128)(2,1)S(1)} collective-permute-done((bf16[128,512]{1,0:T(8,128)(2,1)S(1)}, bf16[128,512]{1,0:T(8,128)(2,1)S(1)}, u32[]{:S(2)}, u32[]{:S(2)}) %collective-permute-start.5) | collective-permute-done | bytes 131104 | tf_op jit(solution)/shard_map/ppermute | solution.py:22
  372.3 2.1 collective-permute-start.6
  374.4 6.2 %collective-permute-done.12 = bf16[128,512]{1,0:T(8,128)(2,1)S(1)} collective-permute-done((bf16[128,512]{1,0:T(8,128)(2,1)S(1)}, bf16[128,512]{1,0:T(8,128)(2,1)S(1)}, u32[]{:S(2)}, u32[]{:S(2)}) %collective-permute-start.12) | collective-permute-done | bytes 131104 | tf_op jit(solution)/shard_map/ppermute | solution.py:24
  381.2 4.4 collective-permute-done.6
  385.7 2.2 collective-permute-start.7
  387.9 6.3 %collective-permute-done.13 = bf16[128,512]{1,0:T(8,128)(2,1)S(1)} collective-permute-done((bf16[128,512]{1,0:T(8,128)(2,1)S(1)}, bf16[128,512]{1,0:T(8,128)(2,1)S(1)}, u32[]{:S(2)}, u32[]{:S(2)}) %collective-permute-start.13) | collective-permute-done | bytes 131104 | tf_op jit(solution)/shard_map/ppermute | solution.py:24
  394.9 6.2 %collective-permute-done.7 = bf16[128,512]{1,0:T(8,128)(2,1)S(1)} collective-permute-done((bf16[128,512]{1,0:T(8,128)(2,1)S(1)}, bf16[128,512]{1,0:T(8,128)(2,1)S(1)}, u32[]{:S(2)}, u32[]{:S(2)}) %collective-permute-start.7) | collective-permute-done | bytes 131104 | tf_op jit(solution)/shard_map/ppermute | solution.py:22
  402.3 6.3 %collective-permute-done.14 = bf16[128,512]{1,0:T(8,128)(2,1)} collective-permute-done((bf16[128,512]{1,0:T(8,128)(2,1)S(1)}, bf16[128,512]{1,0:T(8,128)(2,1)}, u32[]{:S(2)}, u32[]{:S(2)}) %collective-permute-start.14) | collective-permute-done | bytes 131104 | tf_op jit(solution)/shard_map/ppermute | solution.py:24
  408.6 8.0 %collective-permute-done.8 = bf16[128,512]{1,0:T(8,128)(2,1)} collective-permute-done((bf16[128,512]{1,0:T(8,128)(2,1)S(1)}, bf16[128,512]{1,0:T(8,128)(2,1)}, u32[]{:S(2)}, u32[]{:S(2)}) %collective-permute-start.8) | collective-permute-done | bytes 131104 | tf_op jit(solution)/shard_map/ppermute | solution.py:22
  416.6 6.2 %collective-permute-done.15 = bf16[128,512]{1,0:T(8,128)(2,1)} collective-permute-done((bf16[128,512]{1,0:T(8,128)(2,1)}, bf16[128,512]{1,0:T(8,128)(2,1)}, u32[]{:S(2)}, u32[]{:S(2)}) %collective-permute-start.15) | collective-permute-done | bytes 131104 | tf_op jit(solution)/shard_map/ppermute | solution.py:24
  422.8 6.0 %collective-permute-done.9 = bf16[128,512]{1,0:T(8,128)(2,1)} collective-permute-done((bf16[128,512]{1,0:T(8,128)(2,1)}, bf16[128,512]{1,0:T(8,128)(2,1)}, u32[]{:S(2)}, u32[]{:S(2)}) %collective-permute-start.9) | collective-permute-done | bytes 131104 | tf_op jit(solution)/shard_map/ppermute | solution.py:22
  428.8 2.4 collective-permute-start.10
  431.2 6.8 %collective-permute-done.16 = bf16[128,512]{1,0:T(8,128)(2,1)S(1)} collective-permute-done((bf16[128,512]{1,0:T(8,128)(2,1)}, bf16[128,512]{1,0:T(8,128)(2,1)S(1)}, u32[]{:S(2)}, u32[]{:S(2)}) %collective-permute-start.16) | collective-permute-done | bytes 131104 | tf_op jit(solution)/shard_map/ppermute | solution.py:24
  438.0 5.6 collective-permute-done.10
  444.3 1.6 bitcast_dynamic-update-slice_fusion.14
  445.8 1.6 bitcast_dynamic-update-slice_fusion.13
  447.4 1.6 bitcast_dynamic-update-slice_fusion.12
  449.0 1.6 bitcast_dynamic-update-slice_fusion.11
  452.1 1.6 bitcast_dynamic-update-slice_fusion.9
  458.6 1.6 bitcast_dynamic-update-slice_fusion.2
  461.5 3.6 gather_fusion
  465.1 3.1 fusion.21
  468.2 4.7 convolution_convert_fusion
  472.9 2.3 copy.30
  475.2 4.6 all-to-all-start.4
  479.8 1.7 all-to-all-done.4
  482.7 77.6 %reduce-scatter.2.cloned.1.call-done = bf16[128,2048]{1,0:T(8,128)(2,1)} async-done(((bf16[2048,2048]{1,0:T(8,128)(2,1)}), bf16[128,2048]{1,0:T(8,128)(2,1)}) %reduce-scatter.2.cloned.1.call-update) | async-done | bytes 524304 | tf_op jit(solution)/shard_map/reduce_scatter | solution.py:118
  561.4 4.8 all_to_all.55
  568.5 3.0 copy.53
  571.5 3.2 copy.54
  (96 shorter events, 28.2 us)
Async XLA Ops:
  7.2 196.2 %copy-start = (f32[256,6]{0,1:T(8,128)S(1)}, f32[256,6]{0,1:T(8,128)}, u32[]{:S(2)}) copy-start(f32[256,6]{0,1:T(8,128)} %param.12) | copy-start | bytes 18436
  7.2 275.6 %all-gather.5.cloned.1.call-start = ((), (), s32[]{:S(2)}) async-start(), calls=%async_computation.6 | async-start | bytes 8912896 | tf_op jit(solution)/shard_map/all_gather | solution.py:62
  8.7 2.4 copy-start.18
  103.2 5.2 copy-start.6
  103.2 91.6 %all-to-all-start.1 = ((bf16[16,128,512]{2,1,0:T(8,128)(2,1)}), bf16[16,128,512]{2,1,0:T(8,128)(2,1)}, u32[]{:S(2)}, u32[]{:S(2)}) async-start(bf16[16,128,512]{2,1,0:T(8,128)(2,1)} %get-tuple-element.7), calls=%async_computation.1 | async-start | bytes 4194304 | tf_op jit(solution)/shard_map/all_to_all | solution.py:72
  108.3 356.8 %all-gather.7.cloned.1.call-start = ((), (), s32[]{:S(2)}) async-start(), calls=%async_computation.8 | async-start | bytes 2228224 | tf_op jit(solution)/shard_map/all_gather | solution.py:76
  114.0 89.4 %copy-start.17 = (s32[256,6]{0,1:T(8,128)S(1)}, s32[256,6]{0,1:T(8,128)}, u32[]{:S(2)}) copy-start(s32[256,6]{0,1:T(8,128)} %param.11) | copy-start | bytes 18436
  194.8 87.8 %all-to-all-start.2 = ((bf16[16,128,512]{2,1,0:T(8,128)(2,1)}), bf16[16,128,512]{2,1,0:T(8,128)(2,1)}, u32[]{:S(2)}, u32[]{:S(2)}) async-start(bf16[16,128,512]{2,1,0:T(8,128)(2,1)} %convert_element_type.59), calls=%async_computation.2 | async-start | bytes 4194304 | tf_op jit(solution)/shard_map/all_to_all | solution.py:73
  202.2 266.0 %all-gather.9.cloned.1.call-start = ((), (), s32[]{:S(2)}) async-start(), calls=%async_computation.9 | async-start | bytes 2228224 | tf_op jit(solution)/shard_map/all_gather | solution.py:79
  202.2 90.2 %collective-permute-start = (bf16[2048,512]{1,0:T(8,128)(2,1)S(1)}, bf16[2048,512]{1,0:T(8,128)(2,1)}, u32[]{:S(2)}, u32[]{:S(2)}) collective-permute-start(bf16[2048,512]{1,0:T(8,128)(2,1)S(1)} %bitcast.75), channel_id=1, source_target_pairs={{0,1},{1,0},{2,3},{3,2},{4,5},{5,4},{6,7},{7,6},{8,9},{9,8},{10,11... | collective-permute-start | bytes 6291464 | tf_op jit(solution)/shard_map/ppermute | solution.py:109
  203.4 357.0 %reduce-scatter.2.cloned.1.call-start = ((), (), s32[]{:S(2)}) async-start(), calls=%async_computation.7 | async-start | bytes 8912896 | tf_op jit(solution)/shard_map/reduce_scatter | solution.py:118
  275.8 24.3 %collective-permute-start.1 = (bf16[2048,512]{1,0:T(8,128)(2,1)}, bf16[2048,512]{1,0:T(8,128)(2,1)}, u32[]{:S(2)}, u32[]{:S(2)}) collective-permute-start(bf16[2048,512]{1,0:T(8,128)(2,1)} %bitcast.1), channel_id=1, source_target_pairs={{0,1},{1,0},{2,3},{3,2},{4,5},{5,4},{6,7},{7,6},{8,9},{9,8},{10,11... | collective-permute-start | bytes 6291464 | tf_op jit(solution)/shard_map/ppermute | solution.py:110
  282.7 41.7 %collective-permute-start.2 = (bf16[2048,512]{1,0:T(8,128)(2,1)}, bf16[2048,512]{1,0:T(8,128)(2,1)}, u32[]{:S(2)}, u32[]{:S(2)}) collective-permute-start(bf16[2048,512]{1,0:T(8,128)(2,1)} %bitcast.4), channel_id=1, source_target_pairs={{0,1},{1,0},{2,3},{3,2},{4,5},{5,4},{6,7},{7,6},{8,9},{9,8},{10,11... | collective-permute-start | bytes 6291464 | tf_op jit(solution)/shard_map/ppermute | solution.py:111
  282.8 9.7 %copy-start.19 = (bf16[2048,2048]{1,0:T(8,128)(2,1)S(1)}, bf16[2048,2048]{1,0:T(8,128)(2,1)}, u32[]{:S(2)}) copy-start(bf16[2048,2048]{1,0:T(8,128)(2,1)} %all-gather.5.cloned.1.call-done) | copy-start | bytes 25165828
  337.9 0.9 copy-start.5
  338.9 4.7 collective-permute-start.3
  343.6 17.9 %collective-permute-start.4 = (bf16[128,512]{1,0:T(8,128)(2,1)S(1)}, bf16[128,512]{1,0:T(8,128)(2,1)S(1)}, u32[]{:S(2)}, u32[]{:S(2)}) collective-permute-start(bf16[128,512]{1,0:T(8,128)(2,1)S(1)} %collective-permute-done.3), channel_id=1, source_target_pairs={{0,2},{2,4},{4,6},{6,8},{8,10},{10,12},{12,14},{14,16},{16,18},{18... | collective-permute-start | bytes 393224 | tf_op jit(solution)/shard_map/ppermute | solution.py:22
  346.2 15.3 %collective-permute-start.11 = (bf16[128,512]{1,0:T(8,128)(2,1)S(1)}, bf16[128,512]{1,0:T(8,128)(2,1)S(1)}, u32[]{:S(2)}, u32[]{:S(2)}) collective-permute-start(bf16[128,512]{1,0:T(8,128)(2,1)S(1)} %convert_element_type.68), channel_id=1, source_target_pairs={{2,0},{4,2},{6,4},{8,6},{10,8},{12,10},{14,12},{16,14},{18,16},{20... | collective-permute-start | bytes 393224 | tf_op jit(solution)/shard_map/ppermute | solution.py:24
  361.5 19.0 %copy-start.9 = (bf16[128,512]{1,0:T(8,128)(2,1)}, bf16[128,512]{1,0:T(8,128)(2,1)S(1)}, u32[]{:S(2)}) copy-start(bf16[128,512]{1,0:T(8,128)(2,1)S(1)} %collective-permute-done.4) | copy-start | bytes 393220
  361.5 10.8 %collective-permute-start.5 = (bf16[128,512]{1,0:T(8,128)(2,1)S(1)}, bf16[128,512]{1,0:T(8,128)(2,1)S(1)}, u32[]{:S(2)}, u32[]{:S(2)}) collective-permute-start(bf16[128,512]{1,0:T(8,128)(2,1)S(1)} %collective-permute-done.4), channel_id=1, source_target_pairs={{0,2},{2,4},{4,6},{6,8},{8,10},{10,12},{12,14},{14,16},{16,18},{18... | collective-permute-start | bytes 393224 | tf_op jit(solution)/shard_map/ppermute | solution.py:22
  361.5 0.7 copy-start.7
  362.2 18.3 %collective-permute-start.12 = (bf16[128,512]{1,0:T(8,128)(2,1)S(1)}, bf16[128,512]{1,0:T(8,128)(2,1)S(1)}, u32[]{:S(2)}, u32[]{:S(2)}) collective-permute-start(bf16[128,512]{1,0:T(8,128)(2,1)S(1)} %collective-permute-done.11), channel_id=1, source_target_pairs={{2,0},{4,2},{6,4},{8,6},{10,8},{12,10},{14,12},{16,14},{18,16},{20... | collective-permute-start | bytes 393224 | tf_op jit(solution)/shard_map/ppermute | solution.py:24
  372.3 21.9 %copy-start.12 = (bf16[128,512]{1,0:T(8,128)(2,1)}, bf16[128,512]{1,0:T(8,128)(2,1)S(1)}, u32[]{:S(2)}) copy-start(bf16[128,512]{1,0:T(8,128)(2,1)S(1)} %collective-permute-done.5) | copy-start | bytes 393220
  372.3 13.3 %collective-permute-start.6 = (bf16[128,512]{1,0:T(8,128)(2,1)S(1)}, bf16[128,512]{1,0:T(8,128)(2,1)S(1)}, u32[]{:S(2)}, u32[]{:S(2)}) collective-permute-start(bf16[128,512]{1,0:T(8,128)(2,1)S(1)} %collective-permute-done.5), channel_id=1, source_target_pairs={{0,2},{2,4},{4,6},{6,8},{8,10},{10,12},{12,14},{14,16},{16,18},{18... | collective-permute-start | bytes 393224 | tf_op jit(solution)/shard_map/ppermute | solution.py:22
  380.6 0.7 copy-start.10
  380.6 13.7 %collective-permute-start.13 = (bf16[128,512]{1,0:T(8,128)(2,1)S(1)}, bf16[128,512]{1,0:T(8,128)(2,1)S(1)}, u32[]{:S(2)}, u32[]{:S(2)}) collective-permute-start(bf16[128,512]{1,0:T(8,128)(2,1)S(1)} %collective-permute-done.12), channel_id=1, source_target_pairs={{2,0},{4,2},{6,4},{8,6},{10,8},{12,10},{14,12},{16,14},{18,16},{20... | collective-permute-start | bytes 393224 | tf_op jit(solution)/shard_map/ppermute | solution.py:24
  385.7 22.9 %copy-start.15 = (bf16[128,512]{1,0:T(8,128)(2,1)}, bf16[128,512]{1,0:T(8,128)(2,1)S(1)}, u32[]{:S(2)}) copy-start(bf16[128,512]{1,0:T(8,128)(2,1)S(1)} %collective-permute-done.6) | copy-start | bytes 393220
  385.7 15.4 %collective-permute-start.7 = (bf16[128,512]{1,0:T(8,128)(2,1)S(1)}, bf16[128,512]{1,0:T(8,128)(2,1)S(1)}, u32[]{:S(2)}, u32[]{:S(2)}) collective-permute-start(bf16[128,512]{1,0:T(8,128)(2,1)S(1)} %collective-permute-done.6), channel_id=1, source_target_pairs={{0,2},{2,4},{4,6},{6,8},{8,10},{10,12},{12,14},{14,16},{16,18},{18... | collective-permute-start | bytes 393224 | tf_op jit(solution)/shard_map/ppermute | solution.py:22
  394.2 0.7 copy-start.13
  394.2 14.4 %collective-permute-start.14 = (bf16[128,512]{1,0:T(8,128)(2,1)S(1)}, bf16[128,512]{1,0:T(8,128)(2,1)}, u32[]{:S(2)}, u32[]{:S(2)}) collective-permute-start(bf16[128,512]{1,0:T(8,128)(2,1)S(1)} %collective-permute-done.13), channel_id=1, source_target_pairs={{2,0},{4,2},{6,4},{8,6},{10,8},{12,10},{14,12},{16,14},{18,16},{20... | collective-permute-start | bytes 393224 | tf_op jit(solution)/shard_map/ppermute | solution.py:24
  401.0 7.6 %copy-start.16 = (bf16[128,512]{1,0:T(8,128)(2,1)}, bf16[128,512]{1,0:T(8,128)(2,1)S(1)}, u32[]{:S(2)}) copy-start(bf16[128,512]{1,0:T(8,128)(2,1)S(1)} %collective-permute-done.7) | copy-start | bytes 393220
  401.0 15.5 %collective-permute-start.8 = (bf16[128,512]{1,0:T(8,128)(2,1)S(1)}, bf16[128,512]{1,0:T(8,128)(2,1)}, u32[]{:S(2)}, u32[]{:S(2)}) collective-permute-start(bf16[128,512]{1,0:T(8,128)(2,1)S(1)} %collective-permute-done.7), channel_id=1, source_target_pairs={{0,2},{2,4},{4,6},{6,8},{8,10},{10,12},{12,14},{14,16},{16,18},{18... | collective-permute-start | bytes 393224 | tf_op jit(solution)/shard_map/ppermute | solution.py:22
  408.6 14.2 %collective-permute-start.15 = (bf16[128,512]{1,0:T(8,128)(2,1)}, bf16[128,512]{1,0:T(8,128)(2,1)}, u32[]{:S(2)}, u32[]{:S(2)}) collective-permute-start(bf16[128,512]{1,0:T(8,128)(2,1)} %collective-permute-done.14), channel_id=1, source_target_pairs={{2,0},{4,2},{6,4},{8,6},{10,8},{12,10},{14,12},{16,14},{18,16},{20... | collective-permute-start | bytes 393224 | tf_op jit(solution)/shard_map/ppermute | solution.py:24
  416.6 12.2 %collective-permute-start.9 = (bf16[128,512]{1,0:T(8,128)(2,1)}, bf16[128,512]{1,0:T(8,128)(2,1)}, u32[]{:S(2)}, u32[]{:S(2)}) collective-permute-start(bf16[128,512]{1,0:T(8,128)(2,1)} %collective-permute-done.8), channel_id=1, source_target_pairs={{0,2},{2,4},{4,6},{6,8},{8,10},{10,12},{12,14},{14,16},{16,18},{18... | collective-permute-start | bytes 393224 | tf_op jit(solution)/shard_map/ppermute | solution.py:22
  416.6 38.4 %copy-start.8 = (bf16[128,512]{1,0:T(8,128)(2,1)S(1)}, bf16[128,512]{1,0:T(8,128)(2,1)}, u32[]{:S(2)}) copy-start(bf16[128,512]{1,0:T(8,128)(2,1)} %copy-done.7) | copy-start | bytes 393220
  416.6 39.1 %copy-start.11 = (bf16[128,512]{1,0:T(8,128)(2,1)S(1)}, bf16[128,512]{1,0:T(8,128)(2,1)}, u32[]{:S(2)}) copy-start(bf16[128,512]{1,0:T(8,128)(2,1)} %copy-done.10) | copy-start | bytes 393220
  416.6 39.8 %copy-start.14 = (bf16[128,512]{1,0:T(8,128)(2,1)S(1)}, bf16[128,512]{1,0:T(8,128)(2,1)}, u32[]{:S(2)}) copy-start(bf16[128,512]{1,0:T(8,128)(2,1)} %copy-done.13) | copy-start | bytes 393220
  422.8 15.2 %collective-permute-start.16 = (bf16[128,512]{1,0:T(8,128)(2,1)}, bf16[128,512]{1,0:T(8,128)(2,1)S(1)}, u32[]{:S(2)}, u32[]{:S(2)}) collective-permute-start(bf16[128,512]{1,0:T(8,128)(2,1)} %collective-permute-done.15), channel_id=1, source_target_pairs={{2,0},{4,2},{6,4},{8,6},{10,8},{12,10},{14,12},{16,14},{18,16},{20... | collective-permute-start | bytes 393224 | tf_op jit(solution)/shard_map/ppermute | solution.py:24
  428.8 14.8 %collective-permute-start.10 = (bf16[128,512]{1,0:T(8,128)(2,1)}, bf16[128,512]{1,0:T(8,128)(2,1)S(1)}, u32[]{:S(2)}, u32[]{:S(2)}) collective-permute-start(bf16[128,512]{1,0:T(8,128)(2,1)} %collective-permute-done.9), channel_id=1, source_target_pairs={{0,2},{2,4},{4,6},{6,8},{8,10},{10,12},{12,14},{14,16},{16,18},{18... | collective-permute-start | bytes 393224 | tf_op jit(solution)/shard_map/ppermute | solution.py:22
  438.0 22.8 %collective-permute-start.17 = (bf16[128,512]{1,0:T(8,128)(2,1)S(1)}, bf16[128,512]{1,0:T(8,128)(2,1)S(1)}, u32[]{:S(2)}, u32[]{:S(2)}) collective-permute-start(bf16[128,512]{1,0:T(8,128)(2,1)S(1)} %collective-permute-done.16), channel_id=1, source_target_pairs={{2,0},{4,2},{6,4},{8,6},{10,8},{12,10},{14,12},{16,14},{18,16},{20... | collective-permute-start | bytes 393224 | tf_op jit(solution)/shard_map/ppermute | solution.py:24
  475.2 6.4 %all-to-all-start.4 = ((bf16[2,256,1024]{2,1,0:T(8,128)(2,1)}), bf16[2,256,1024]{2,1,0:T(8,128)(2,1)S(1)}, u32[]{:S(2)}, u32[]{:S(2)}) async-start(bf16[2,256,1024]{2,1,0:T(8,128)(2,1)} %bitcast.78), calls=%async_computation.5 | async-start | bytes 2097152 | tf_op jit(solution)/shard_map/all_to_all | solution.py:90
  482.7 83.5 %copy-start.2 = (f32[256,1024]{1,0:T(8,128)S(1)}, f32[256,1024]{1,0:T(8,128)}, u32[]{:S(2)}) copy-start(f32[256,1024]{1,0:T(8,128)} %convert_reduce_fusion) | copy-start | bytes 3145732
  571.5 3.2 copy-start.3
  574.7 2.3 copy-start.4
  574.7 3.7 copy-start.1
Sparse Core Ops, SparseCore 0:
  11.3 181.4 all-gather.4
  195.6 81.2 all-gather.6
  279.7 59.4 all-gather.8
  341.3 218.9 reduce-scatter.1
